TPU v7x, 32 devices: a whole 2x2x4 slice. The times are simulated.
32 devices in a mesh: sp: 16 (over z, y, x), tp: 2 (over core).
Axes of the slice: x: 2, y: 2, z: 4, core: 2. Of those that a mesh axis runs over, the one named last changes fastest.
Arguments:
- residual: bfloat16 [3072, 2048], P(('sp', 'tp')), may hold values from -6 to 6
- queries_narrow: bfloat16 [3072, 512], P('sp', 'tp'), may hold values from -24 to 24
- keys_narrow: bfloat16 [3072, 512], P('sp', 'tp'), may hold values from -24 to 24
- values_narrow: bfloat16 [3072, 512], P('sp', 'tp'), may hold values from -6 to 6
- queries_broad: bfloat16 [3072, 512], P('sp', 'tp'), may hold values from -24 to 24
- keys_broad: bfloat16 [3072, 512], P('sp', 'tp'), may hold values from -24 to 24
- values_broad: bfloat16 [3072, 512], P('sp', 'tp'), may hold values from -6 to 6
- gates_narrow: float32 [3072, 16], P('sp', 'tp'), may hold values from -3072 to 0, as said below
- gates_broad: float32 [3072, 8], P('sp', 'tp'), may hold values from -3072 to 0, as said below
- project_narrow: bfloat16 [512, 2048], P('tp'), may hold values from -0.5 to 0.5
- project_broad: bfloat16 [512, 2048], P('tp'), may hold values from -0.5 to 0.5
- norm_gain: float32 [2048], replicated, may hold values from 0.1 to 1.9
- up_weight: bfloat16 [2048, 8192], P('sp', 'tp'), may hold values from -0.125 to 0.125
- down_weight: bfloat16 [8192, 2048], P('tp', 'sp'), may hold values from -0.0625 to 0.0625
Outputs:
- layer_out: bfloat16 [3072, 2048], P(('sp', 'tp'))
Inputs may be any that keep to these rules, and one draw needn't show every extreme that they name: `gates_narrow`: each head's cumulative log gate never rises from one position to the next. `gates_broad`: each head's cumulative log gate never rises from one position to the next.
All inputs are finite; a program needn't handle non-finite values.
Results may differ from a plain program's by a relative error of at most 0.018.
Values may be sent and summed in bfloat16 or wider, within the bound.
A program may use at most 128 MiB of HBM per device.

v0:
```python
import jax
import jax.numpy as jnp
from jax import lax
from jax.sharding import PartitionSpec as P

A_DIM = 32
B_DIM = 64


def group_update(state, queries, keys, values, query_gates, key_gates, allowed, head_size):
    peak, total, summed = state
    query_count = queries.shape[0]
    key_count = keys.shape[0]
    heads = queries.shape[1] // head_size
    scores = jnp.einsum(
        "qhd,khd->hqk",
        queries.reshape(query_count, heads, head_size),
        keys.reshape(key_count, heads, head_size),
        preferred_element_type=jnp.float32,
    ) * head_size ** (-0.5)
    scores = scores + query_gates.T[:, :, None] - key_gates.T[:, None, :]
    scores = jnp.where(allowed[None], scores, -1e30)
    new_peak = jnp.maximum(peak, jnp.max(scores, axis=-1))
    weights = jnp.exp(scores - new_peak[..., None]) * allowed[None].astype(jnp.float32)
    total = jnp.sum(weights, axis=-1)
    summed = jnp.einsum(
        "hqk,khd->hqd",
        weights.astype(jnp.bfloat16),
        values.reshape(key_count, heads, head_size),
        preferred_element_type=jnp.float32,
    )
    return (new_peak, total, summed)


def empty_state(query_count, heads, head_size):
    return (
        jnp.full((heads, query_count), -1e30, jnp.float32),
        jnp.zeros((heads, query_count), jnp.float32),
        jnp.zeros((heads, query_count, head_size), jnp.float32),
    )


def finish_group(state, head_size):
    peak, total, summed = state
    result = summed / total[..., None]
    return (
        result.transpose(1, 0, 2)
        .reshape(result.shape[1], result.shape[0] * head_size)
        .astype(jnp.bfloat16)
    )


def rms_scaled(mixed, norm_gain):
    mixed_wide = mixed.astype(jnp.float32)
    scale = lax.rsqrt(jnp.mean(mixed_wide * mixed_wide, axis=-1, keepdims=True) + 1e-06)
    return (mixed_wide * scale * norm_gain).astype(jnp.bfloat16)


def local(
    residual,
    queries_narrow,
    keys_narrow,
    values_narrow,
    queries_broad,
    keys_broad,
    values_broad,
    gates_narrow,
    gates_broad,
    project_narrow,
    project_broad,
    norm_gain,
    up_weight,
    down_weight,
):
    local_count = queries_narrow.shape[0]
    table_narrow, table_broad = (
        lax.all_gather(gates_narrow, "sp", axis=0, tiled=True),
        lax.all_gather(gates_broad, "sp", axis=0, tiled=True),
    )
    query_pos = lax.axis_index("sp") * local_count + jnp.arange(local_count, dtype=jnp.int32)
    initial = (
        empty_state(local_count, queries_narrow.shape[1] // A_DIM, A_DIM),
        empty_state(local_count, queries_broad.shape[1] // B_DIM, B_DIM),
    )
    piece_keys_narrow = lax.all_gather(keys_narrow, "sp", axis=0, tiled=True)
    piece_values_narrow = lax.all_gather(values_narrow, "sp", axis=0, tiled=True)
    piece_keys_broad = lax.all_gather(keys_broad, "sp", axis=0, tiled=True)
    piece_values_broad = lax.all_gather(values_broad, "sp", axis=0, tiled=True)
    piece_count = piece_keys_narrow.shape[0]
    key_pos = jnp.arange(piece_count, dtype=jnp.int32)
    allowed = key_pos[None, :] <= query_pos[:, None]
    state_narrow = group_update(
        initial[0],
        queries_narrow,
        piece_keys_narrow,
        piece_values_narrow,
        gates_narrow,
        table_narrow,
        allowed,
        A_DIM,
    )
    state_broad = group_update(
        initial[1],
        queries_broad,
        piece_keys_broad,
        piece_values_broad,
        gates_broad,
        table_broad,
        allowed,
        B_DIM,
    )
    attended_narrow = finish_group(state_narrow, A_DIM)
    attended_broad = finish_group(state_broad, B_DIM)
    projected = lax.psum_scatter(
        (
            jnp.dot(attended_narrow, project_narrow, preferred_element_type=jnp.float32)
            + jnp.dot(attended_broad, project_broad, preferred_element_type=jnp.float32)
        ).astype(jnp.bfloat16),
        "tp",
        scatter_dimension=0,
        tiled=True,
    ).astype(jnp.float32)
    mixed = (residual.astype(jnp.float32) + projected).astype(jnp.bfloat16)
    features = lax.all_gather(rms_scaled(mixed, norm_gain), "tp", axis=0, tiled=True)
    up_total = jnp.dot(
        features,
        lax.all_gather(up_weight, "sp", axis=0, tiled=True),
        preferred_element_type=jnp.float32,
    )
    hidden = jnp.square(jax.nn.relu(up_total)).astype(jnp.bfloat16)
    down_term = jnp.dot(
        hidden,
        lax.all_gather(down_weight, "sp", axis=1, tiled=True),
        preferred_element_type=jnp.float32,
    )
    summed_rows = lax.psum_scatter(
        down_term.astype(jnp.bfloat16), "tp", scatter_dimension=0, tiled=True
    ).astype(jnp.float32)
    return (mixed.astype(jnp.float32) + summed_rows).astype(jnp.bfloat16)


def solution(mesh):
    return jax.shard_map(
        local,
        mesh=mesh,
        in_specs=(
            P(("sp", "tp"), None),
            P("sp", "tp"),
            P("sp", "tp"),
            P("sp", "tp"),
            P("sp", "tp"),
            P("sp", "tp"),
            P("sp", "tp"),
            P("sp", "tp"),
            P("sp", "tp"),
            P("tp", None),
            P("tp", None),
            P(),
            P("sp", "tp"),
            P("tp", "sp"),
        ),
        out_specs=P(("sp", "tp"), None),
        check_vma=False,
    )
```

profile of v0, /device:TPU:0, one launch (start us, length us, event | category | flops | bytes accessed | tf_op | source)
XLA Modules:
  0.0 742.3 jit_solution(3498710460941625432)
XLA Ops:
  6.5 0.7 all-gather.9.cloned.1.call-update
  7.3 0.0 all-gather.13.cloned.1.call-start
  7.3 0.7 all-gather.13.cloned.1.call-update
  8.0 0.0 all-gather.11.cloned.1.call-start
  8.1 0.7 all-gather.11.cloned.1.call-update
  8.7 0.0 all-gather.15.cloned.1.call-start
  8.8 0.5 all-gather.15.cloned.1.call-update
  9.3 0.0 reduce-scatter.3.cloned.1.call-start
  9.4 1.3 iota_compare_fusion
  10.7 43.5 %all-gather = f32[16,192,8]{1,2,0:T(8,128)S(1)} all-gather(f32[1,192,8]{1,2,0:T(8,128)} %bitcast.59), channel_id=1, replica_groups=mesh['sp'=16,'tp'=2] {'sp'}, dimensions={0}, use_global_device_ids=true | all-gather | bytes 104448 | tf_op jit(solution)/shard_map/all_gather | solution.py:77
  54.3 0.7 reshape.92
  55.0 1.7 copy.29
  56.7 36.3 %all-gather.1 = f32[16,192,4]{1,2,0:T(4,128)S(1)} all-gather(f32[1,192,4]{1,2,0:T(4,128)} %bitcast.65), channel_id=1, replica_groups=mesh['sp'=16,'tp'=2] {'sp'}, dimensions={0}, use_global_device_ids=true | all-gather | bytes 52224 | tf_op jit(solution)/shard_map/all_gather | solution.py:78
  93.0 0.1 reshape.94
  93.1 1.6 copy.33
  94.7 2.6 copy.30
  97.3 7.4 fusion.2
  104.8 6.4 copy-done.4
  111.2 0.4 copy-done.14
  111.5 8.6 %fusion = f32[8,192]{1,0:T(8,128)} fusion(f32[8,192,3072]{2,1,0:T(8,128)S(1)} %get-tuple-element.8, f32[192,3072]{1,0:T(8,128)S(1)} %get-tuple-element.6, f32[8,192]{1,0:T(8,128)S(1)} %broadcast_maximum_fusion, f32[8,3072]{1,0:T(8,128)S(1)} %bitcast.53, f32[8,192]{1,0:T(8,128)S(1)} %bitcast.61, pred[192,3072]{1,0:T(8,128)(4,1)S(1)} %copy-done.8), kind=kLoop, calls=%fused_computation.2 | loop fusion | flops 33028608 | bytes 21940224 | tf_op jit(solution)/shard_map/reduce_sum | solution.py:25
  120.2 10.4 %all-gather.13.cloned.1.call-done = bf16[3072,256]{1,0:T(8,128)(2,1)} async-done(((bf16[192,256]{1,0:T(8,128)(2,1)}), bf16[3072,256]{1,0:T(8,128)(2,1)}) %all-gather.13.cloned.1.call-update) | async-done | bytes 1572880 | tf_op jit(solution)/shard_map/all_gather | solution.py:87
  130.6 2.6 copy.34
  133.2 8.0 %fusion.41 = (f32[4,192]{1,0:T(4,128)S(1)}, f32[4,192,3072]{2,1,0:T(8,128)}) fusion(f32[4,3072]{1,0:T(4,128)S(1)} %bitcast.58, f32[4,192]{1,0:T(4,128)} %bitcast.66, bf16[192,4,64]{0,2,1:T(8,128)(2,1)} %bitcast.55, bf16[3072,4,64]{0,2,1:T(8,128)(2,1)} %bitcast.49, pred[192,3072]{1,0:T(8,128)(4,1)} %get-tuple-element.5), kind=kOutput, calls=%fused_computation.43 | convolution fusion | flops 313785600 | bytes 11753472 | tf_op jit(solution)/shard_map/qhd,khd->hqk/dot_general | solution.py:15
  141.1 48.9 %all-gather.11.cloned.1.call-done = bf16[3072,256]{1,0:T(8,128)(2,1)} async-done(((bf16[192,256]{1,0:T(8,128)(2,1)}), bf16[3072,256]{1,0:T(8,128)(2,1)}) %all-gather.11.cloned.1.call-update) | async-done | bytes 1572880 | tf_op jit(solution)/shard_map/all_gather | solution.py:86
  190.1 2.7 copy.32
  192.8 11.0 %fusion.24 = bf16[192,8,32]{0,2,1:T(8,128)(2,1)S(1)} fusion(bf16[3072,8,32]{0,2,1:T(8,128)(2,1)} %bitcast.48, f32[8,192,3072]{2,1,0:T(8,128)} %copy-done.4, f32[192,3072]{1,0:T(8,128)} %copy-done.2, f32[8,192]{1,0:T(8,128)S(1)} %copy-done.15, f32[8,3072]{1,0:T(8,128)S(1)} %bitcast.54, f32[8,192]{1,0:T(8,128)S(1)} %bitcast.62, ...), kind=kOutput, calls=%fused_computation.27 | convolution fusion | flops 335118336 | bytes 23611392 | tf_op jit(solution)/shard_map/hqk,khd->hqd/dot_general | solution.py:26
  203.8 1.6 fusion.42
  205.4 1.8 fusion.6
  207.3 42.1 %all-gather.15.cloned.1.call-done = bf16[3072,256]{1,0:T(8,128)(2,1)} async-done(((bf16[192,256]{1,0:T(8,128)(2,1)}), bf16[3072,256]{1,0:T(8,128)(2,1)}) %all-gather.15.cloned.1.call-update) | async-done | bytes 1572880 | tf_op jit(solution)/shard_map/all_gather | solution.py:88
  249.4 2.6 copy.36
  252.0 6.7 fusion.30
  258.8 1.3 fusion.14
  260.1 0.0 reduce-scatter.3.cloned.1.call-update
  260.1 0.0 all-gather.17.cloned.1.call-start
  260.2 0.5 all-gather.17.cloned.1.call-update
  260.7 0.0 all-gather.19.cloned.1.call-start
  260.7 0.7 all-gather.19.cloned.1.call-update
  261.4 0.0 reduce-scatter.5.cloned.1.call-start
  261.5 5.7 reduce-scatter.3.cloned.1.call-done
  267.1 1.2 fusion.33
  268.4 1.2 fusion.35
  269.6 2.4 all_gather.33
  271.9 190.0 %all-gather.17.cloned.1.call-done = bf16[2048,4096]{1,0:T(8,128)(2,1)} async-done(((bf16[128,4096]{1,0:T(8,128)(2,1)}), bf16[2048,4096]{1,0:T(8,128)(2,1)}) %all-gather.17.cloned.1.call-update) | async-done | bytes 16777232 | tf_op jit(solution)/shard_map/all_gather | solution.py:127
  461.9 250.0 %all-gather.19.cloned.1.call-done = bf16[4096,2048]{1,0:T(8,128)(2,1)} async-done(((bf16[4096,128]{1,0:T(8,128)(2,1)}), bf16[4096,2048]{1,0:T(8,128)(2,1)}) %all-gather.19.cloned.1.call-update) | async-done | bytes 16777232 | tf_op jit(solution)/shard_map/all_gather | solution.py:133
  711.9 15.1 %convolution_convert_fusion = bf16[192,2048]{1,0:T(8,128)(2,1)} fusion(bf16[4096,2048]{1,0:T(8,128)(2,1)} %all-gather.19.cloned.1.call-done, bf16[192,2048]{1,0:T(8,128)(2,1)S(1)} %all_gather.33, bf16[2048,4096]{1,0:T(8,128)(2,1)} %all-gather.17.cloned.1.call-done), kind=kOutput, calls=%fused_computation.18 | convolution fusion | flops 6445203456 | bytes 35127296 | tf_op jit(solution)/shard_map/dot_general | solution.py:131
  727.0 0.0 reduce-scatter.5.cloned.1.call-update
  727.0 6.5 reduce-scatter.5.cloned.1.call-done
  733.5 1.9 fusion.36
  (49 shorter events, 0.2 us)
Async XLA Ops:
  6.5 197.3 %copy-start = (bf16[256,2048]{1,0:T(8,128)(2,1)S(1)}, bf16[256,2048]{1,0:T(8,128)(2,1)}, u32[]{:S(2)}) copy-start(bf16[256,2048]{1,0:T(8,128)(2,1)} %param.23) | copy-start | bytes 3145732
  6.5 88.2 %all-gather.9.cloned.1.call-start = ((), (), s32[]{:S(2)}) async-start(), calls=%async_computation.2 | async-start | bytes 1671168 | tf_op jit(solution)/shard_map/all_gather | solution.py:85
  7.3 123.3 %all-gather.13.cloned.1.call-start = ((), (), s32[]{:S(2)}) async-start(), calls=%async_computation.4 | async-start | bytes 1671168 | tf_op jit(solution)/shard_map/all_gather | solution.py:87
  8.0 182.0 %all-gather.11.cloned.1.call-start = ((), (), s32[]{:S(2)}) async-start(), calls=%async_computation.3 | async-start | bytes 1671168 | tf_op jit(solution)/shard_map/all_gather | solution.py:86
  8.7 240.7 %all-gather.15.cloned.1.call-start = ((), (), s32[]{:S(2)}) async-start(), calls=%async_computation.5 | async-start | bytes 1671168 | tf_op jit(solution)/shard_map/all_gather | solution.py:88
  9.3 257.8 %reduce-scatter.3.cloned.1.call-start = ((), (), s32[]{:S(2)}) async-start(), calls=%async_computation.6 | async-start | bytes 1179648 | tf_op jit(solution)/shard_map/reduce_scatter | solution.py:114
  10.7 94.0 %copy-start.2 = (f32[192,3072]{1,0:T(8,128)}, f32[192,3072]{1,0:T(8,128)S(1)}, u32[]{:S(2)}) copy-start(f32[192,3072]{1,0:T(8,128)S(1)} %get-tuple-element.6) | copy-start | bytes 7077892
  97.3 14.2 %copy-start.8 = (pred[192,3072]{1,0:T(8,128)(4,1)S(1)}, pred[192,3072]{1,0:T(8,128)(4,1)}, u32[]{:S(2)}) copy-start(pred[192,3072]{1,0:T(8,128)(4,1)} %get-tuple-element.5) | copy-start | bytes 1769476
  97.3 14.2 %copy-start.11 = (f32[3072,8]{0,1:T(8,128)S(1)}, f32[3072,8]{0,1:T(8,128)}, u32[]{:S(2)}) copy-start(f32[3072,8]{0,1:T(8,128)} %reshape.92) | copy-start | bytes 294916
  97.3 14.2 %copy-start.12 = (f32[192,8]{0,1:T(8,128)S(1)}, f32[192,8]{0,1:T(8,128)}, u32[]{:S(2)}) copy-start(f32[192,8]{0,1:T(8,128)} %param.21) | copy-start | bytes 18436
  104.7 6.4 copy-start.4
  104.7 6.8 copy-start.14
  133.2 59.6 %copy-start.9 = (pred[192,3072]{1,0:T(8,128)(4,1)S(1)}, pred[192,3072]{1,0:T(8,128)(4,1)}, u32[]{:S(2)}) copy-start(pred[192,3072]{1,0:T(8,128)(4,1)} %get-tuple-element.5) | copy-start | bytes 1769476
  133.2 59.6 %copy-start.13 = (f32[192,8]{0,1:T(8,128)S(1)}, f32[192,8]{0,1:T(8,128)}, u32[]{:S(2)}) copy-start(f32[192,8]{0,1:T(8,128)} %param.21) | copy-start | bytes 18436
  133.2 59.6 %copy-start.15 = (f32[8,192]{1,0:T(8,128)S(1)}, f32[8,192]{1,0:T(8,128)}, u32[]{:S(2)}) copy-start(f32[8,192]{1,0:T(8,128)} %copy-done.14) | copy-start | bytes 18436
  133.2 59.6 %copy-start.17 = (f32[8,192]{1,0:T(8,128)S(1)}, f32[8,192]{1,0:T(8,128)}, u32[]{:S(2)}) copy-start(f32[8,192]{1,0:T(8,128)} %fusion) | copy-start | bytes 18436
  190.0 15.4 %slice-start = ((s8[9437184]{0:T(1024)(128)(4,1)}), s8[1048576]{0:T(1024)(128)(4,1)S(1)}, s32[]{:S(2)}) async-start(s8[9437184]{0:T(1024)(128)(4,1)} %bitcast.45), calls=%async_computation.10 | async-start | bytes 2097152
  192.8 12.6 %slice-start.1 = ((s8[9437184]{0:T(1024)(128)(4,1)}), s8[4194304]{0:T(1024)(128)(4,1)S(1)}, s32[]{:S(2)}) async-start(s8[9437184]{0:T(1024)(128)(4,1)} %bitcast.45), calls=%async_computation.11 | async-start | bytes 8388608
  192.8 12.6 %slice-start.2 = ((s8[9437184]{0:T(1024)(128)(4,1)}), s8[4194304]{0:T(1024)(128)(4,1)S(1)}, s32[]{:S(2)}) async-start(s8[9437184]{0:T(1024)(128)(4,1)} %bitcast.45), calls=%async_computation.12 | async-start | bytes 8388608
  192.8 12.6 %copy-start.3 = (f32[192,3072]{1,0:T(8,128)S(1)}, f32[192,3072]{1,0:T(8,128)}, u32[]{:S(2)}) copy-start(f32[192,3072]{1,0:T(8,128)} %copy-done.2) | copy-start | bytes 7077892
  207.3 51.5 %copy-start.5 = (f32[192,2048]{1,0:T(8,128)S(1)}, f32[192,2048]{1,0:T(8,128)}, u32[]{:S(2)}) copy-start(f32[192,2048]{1,0:T(8,128)} %fusion.42) | copy-start | bytes 4718596
  207.3 51.5 %copy-start.10 = (bf16[256,2048]{1,0:T(8,128)(2,1)S(1)}, bf16[256,2048]{1,0:T(8,128)(2,1)}, u32[]{:S(2)}) copy-start(bf16[256,2048]{1,0:T(8,128)(2,1)} %param.24) | copy-start | bytes 3145732
  252.0 15.1 %copy-start.6 = (bf16[96,2048]{1,0:T(8,128)(2,1)S(1)}, bf16[96,2048]{1,0:T(8,128)(2,1)}, u32[]{:S(2)}) copy-start(bf16[96,2048]{1,0:T(8,128)(2,1)} %param.14) | copy-start | bytes 1179652
  252.0 16.4 %copy-start.16 = (f32[2048]{0:T(1024)S(1)}, f32[2048]{0:T(1024)}, u32[]{:S(2)}) copy-start(f32[2048]{0:T(1024)} %param.25) | copy-start | bytes 24580
  260.1 201.8 %all-gather.17.cloned.1.call-start = ((), (), s32[]{:S(2)}) async-start(), calls=%async_computation.7 | async-start | bytes 17825792 | tf_op jit(solution)/shard_map/all_gather | solution.py:127
  260.7 451.2 %all-gather.19.cloned.1.call-start = ((), (), s32[]{:S(2)}) async-start(), calls=%async_computation.8 | async-start | bytes 17825792 | tf_op jit(solution)/shard_map/all_gather | solution.py:133
  261.4 472.1 %reduce-scatter.5.cloned.1.call-start = ((), (), s32[]{:S(2)}) async-start(), calls=%async_computation.9 | async-start | bytes 1179648 | tf_op jit(solution)/shard_map/reduce_scatter | solution.py:136
  271.9 461.6 %copy-start.7 = (bf16[96,2048]{1,0:T(8,128)(2,1)S(1)}, bf16[96,2048]{1,0:T(8,128)(2,1)}, u32[]{:S(2)}) copy-start(bf16[96,2048]{1,0:T(8,128)(2,1)} %reduce-scatter.3.cloned.1.call-done) | copy-start | bytes 1179652
  711.9 23.5 %copy-start.1 = (bf16[256,2048]{1,0:T(8,128)(2,1)S(1)}, bf16[256,2048]{1,0:T(8,128)(2,1)}, u32[]{:S(2)}) copy-start(bf16[256,2048]{1,0:T(8,128)(2,1)} %param.23) | copy-start | bytes 3145732
Sparse Core Ops, SparseCore 0:
  10.1 60.9 all-gather.8
  73.8 56.6 all-gather.12
  133.3 56.6 all-gather.10
  192.7 56.7 all-gather.14
  260.2 6.8 reduce-scatter.2
  269.8 192.1 all-gather.16
  464.6 247.2 all-gather.18
  727.2 6.3 reduce-scatter.4
where the time goes:
time: 743 us; the launch traced here: 742 us
  waiting for transfers between devices  557 us (75%)
  blocking collectives  82.2 us (11%)
  matrix products  51.1 us (7%)
  local copies, waits for them, and re-layouts  21.5 us (3%)
  other arithmetic  16.1 us (2%)
  between operations  13.7 us (2%)
    all_gather x1, waiting for transfers between devices, local(): lax.all_gather(down_weight, 'sp', axis=1, tiled=True)  250 us
    all_gather x1, waiting for transfers between devices, local(): lax.all_gather(up_weight, 'sp', axis=0, tiled=True)  190 us
    all_gather x1, waiting for transfers between devices, local(): lax.all_gather(values_narrow, 'sp', axis=0, tiled=True)  48.9 us
    all_gather x1, blocking collectives, local(): lax.all_gather(gates_narrow, 'sp', axis=0, tiled=True)  43.5 us
    all_gather x1, waiting for transfers between devices, local(): piece_values_broad = lax.all_gather(values_broad, 'sp', axis=0, tiled=True)  42.1 us
    all_gather x1, blocking collectives, local(): lax.all_gather(gates_broad, 'sp', axis=0, tiled=True)  36.3 us
    dot_general x2, matrix products, group_update(): jnp.einsum('hqk,khd->hqd', weights.astype(jnp.bfloat16), values.reshape(k...  17.7 us
    dot_general x2, matrix products, group_update(): jnp.einsum('qhd,khd->hqk', queries.reshape(query_count, heads, head_size)...  15.4 us
  transfers between devices with their start and end apart: 8, of which 7 were waited for; matrix products, arithmetic and copies ran while one was open for 7% of the time, Pallas kernels for 0%

commit v1 on v0

--- a/solution.py
+++ b/solution.py
@@ -130,7 +130,9 @@
     hidden = jnp.square(jax.nn.relu(up_total)).astype(jnp.bfloat16)
     down_term = jnp.dot(
         hidden,
-        lax.all_gather(down_weight, "sp", axis=1, tiled=True),
+        jnp.concatenate(
+            lax.all_to_all(jnp.stack([down_weight] * lax.axis_size("sp")), "sp", 0, 0), axis=1
+        ),
         preferred_element_type=jnp.float32,
     )
     summed_rows = lax.psum_scatter(

time: 743 us -> 840 us (1.13)
  waiting for transfers between devices: 557 us -> 641 us
    all_to_all x0 -> x1, waiting for transfers between devices: none -> 367 us  [local(): lax.all_to_all(jnp.stack([down_weight] * lax.axis_size('sp')), 'sp', 0, 0)]
    all_gather x1 -> x0, waiting for transfers between devices: 250 us -> none  [local(): lax.all_gather(down_weight, 'sp', axis=1, tiled=True)]
    all_gather x1, waiting for transfers between devices: 190 us -> 129 us  [local(): lax.all_gather(up_weight, 'sp', axis=0, tiled=True)]
    reduce_scatter x1, waiting for transfers between devices: 6.5 us -> 40.8 us  [local(): lax.psum_scatter(down_term.astype(jnp.bfloat16), 'tp', scatter_dimension=...]
  transfers between devices with their start and end apart: 8 -> 8, of which waited for: 7 -> 6; matrix products, arithmetic and copies ran while one was open for 7% -> 7% of each run, Pallas kernels for 0% -> 0%
where the time goes in v1:
time: 840 us; the launch traced here: 839 us
  waiting for transfers between devices  641 us (76%)
  blocking collectives  82.1 us (10%)
  matrix products  52.2 us (6%)
  local copies, waits for them, and re-layouts  29 us (3%)
  other arithmetic  16.1 us (2%)
  between operations  13.7 us (2%)
    all_to_all x1, waiting for transfers between devices, local(): lax.all_to_all(jnp.stack([down_weight] * lax.axis_size('sp')), 'sp', 0, 0)  367 us
    all_gather x1, waiting for transfers between devices, local(): lax.all_gather(up_weight, 'sp', axis=0, tiled=True)  129 us
    all_gather x1, waiting for transfers between devices, local(): lax.all_gather(values_narrow, 'sp', axis=0, tiled=True)  48.9 us
    all_gather x1, blocking collectives, local(): lax.all_gather(gates_narrow, 'sp', axis=0, tiled=True)  43.5 us
    all_gather x1, waiting for transfers between devices, local(): piece_values_broad = lax.all_gather(values_broad, 'sp', axis=0, tiled=True)  42.1 us
    reduce_scatter x1, waiting for transfers between devices, local(): lax.psum_scatter(down_term.astype(jnp.bfloat16), 'tp', scatter_dimension=...  40.8 us
    all_gather x1, blocking collectives, local(): lax.all_gather(gates_broad, 'sp', axis=0, tiled=True)  36.2 us
    dot_general x2, matrix products, group_update(): jnp.einsum('hqk,khd->hqd', weights.astype(jnp.bfloat16), values.reshape(k...  17.7 us
  transfers between devices with their start and end apart: 8, of which 6 were waited for; matrix products, arithmetic and copies ran while one was open for 7% of the time, Pallas kernels for 0%

profile of v1, /device:TPU:0, one launch (start us, length us, event | category | flops | bytes accessed | tf_op | source)
XLA Modules:
  0.0 839.4 jit_solution(5525758148933709977)
XLA Ops:
  6.5 0.7 all-gather.8.cloned.1.call-update
  7.3 0.0 all-gather.12.cloned.1.call-start
  7.3 0.7 all-gather.12.cloned.1.call-update
  8.0 0.0 all-gather.10.cloned.1.call-start
  8.1 0.7 all-gather.10.cloned.1.call-update
  8.7 0.0 all-gather.14.cloned.1.call-start
  8.8 0.5 all-gather.14.cloned.1.call-update
  9.3 0.0 reduce-scatter.3.cloned.1.call-start
  9.4 1.3 iota_compare_fusion
  10.7 43.5 %all-gather = f32[16,192,8]{1,2,0:T(8,128)S(1)} all-gather(f32[1,192,8]{1,2,0:T(8,128)} %bitcast.62), channel_id=1, replica_groups=mesh['sp'=16,'tp'=2] {'sp'}, dimensions={0}, use_global_device_ids=true | all-gather | bytes 104448 | tf_op jit(solution)/shard_map/all_gather | solution.py:77
  54.3 0.7 reshape.102
  55.0 1.7 copy.30
  56.7 36.2 %all-gather.1 = f32[16,192,4]{1,2,0:T(4,128)S(1)} all-gather(f32[1,192,4]{1,2,0:T(4,128)} %bitcast.68), channel_id=1, replica_groups=mesh['sp'=16,'tp'=2] {'sp'}, dimensions={0}, use_global_device_ids=true | all-gather | bytes 52224 | tf_op jit(solution)/shard_map/all_gather | solution.py:78
  92.9 0.1 reshape.104
  93.0 1.6 copy.34
  94.7 2.6 copy.31
  97.3 7.4 fusion.2
  104.7 6.4 copy-done.4
  111.1 0.4 copy-done.14
  111.5 8.6 %fusion = f32[8,192]{1,0:T(8,128)} fusion(f32[8,192,3072]{2,1,0:T(8,128)S(1)} %get-tuple-element.8, f32[192,3072]{1,0:T(8,128)S(1)} %get-tuple-element.6, f32[8,192]{1,0:T(8,128)S(1)} %broadcast_maximum_fusion, f32[8,3072]{1,0:T(8,128)S(1)} %bitcast.56, f32[8,192]{1,0:T(8,128)S(1)} %bitcast.64, pred[192,3072]{1,0:T(8,128)(4,1)S(1)} %copy-done.8), kind=kLoop, calls=%fused_computation.2 | loop fusion | flops 33028608 | bytes 21940224 | tf_op jit(solution)/shard_map/reduce_sum | solution.py:25
  120.1 10.5 %all-gather.12.cloned.1.call-done = bf16[3072,256]{1,0:T(8,128)(2,1)} async-done(((bf16[192,256]{1,0:T(8,128)(2,1)}), bf16[3072,256]{1,0:T(8,128)(2,1)}) %all-gather.12.cloned.1.call-update) | async-done | bytes 1572880 | tf_op jit(solution)/shard_map/all_gather | solution.py:87
  130.6 2.6 copy.35
  133.2 8.0 fusion.41
  141.2 48.9 %all-gather.10.cloned.1.call-done = bf16[3072,256]{1,0:T(8,128)(2,1)} async-done(((bf16[192,256]{1,0:T(8,128)(2,1)}), bf16[3072,256]{1,0:T(8,128)(2,1)}) %all-gather.10.cloned.1.call-update) | async-done | bytes 1572880 | tf_op jit(solution)/shard_map/all_gather | solution.py:86
  190.1 2.7 copy.33
  192.8 11.0 %fusion.24 = bf16[192,8,32]{0,2,1:T(8,128)(2,1)S(1)} fusion(bf16[3072,8,32]{0,2,1:T(8,128)(2,1)} %bitcast.51, f32[8,192,3072]{2,1,0:T(8,128)} %copy-done.4, f32[192,3072]{1,0:T(8,128)} %copy-done.2, f32[8,192]{1,0:T(8,128)S(1)} %copy-done.15, f32[8,3072]{1,0:T(8,128)S(1)} %bitcast.57, f32[8,192]{1,0:T(8,128)S(1)} %bitcast.65, ...), kind=kOutput, calls=%fused_computation.27 | convolution fusion | flops 335118336 | bytes 23611392 | tf_op jit(solution)/shard_map/hqk,khd->hqd/dot_general | solution.py:26
  203.8 1.6 fusion.42
  205.4 1.8 fusion.6
  207.3 42.1 %all-gather.14.cloned.1.call-done = bf16[3072,256]{1,0:T(8,128)(2,1)} async-done(((bf16[192,256]{1,0:T(8,128)(2,1)}), bf16[3072,256]{1,0:T(8,128)(2,1)}) %all-gather.14.cloned.1.call-update) | async-done | bytes 1572880 | tf_op jit(solution)/shard_map/all_gather | solution.py:88
  249.4 2.6 copy.37
  252.0 6.7 fusion.30
  258.7 1.3 fusion.14
  260.0 0.0 reduce-scatter.3.cloned.1.call-update
  260.1 1.5 copy.38
  261.6 6.0 stack.2
  267.6 5.3 all-to-all-start
  272.9 0.0 all-gather.16.cloned.1.call-start
  272.9 0.5 all-gather.16.cloned.1.call-update
  273.5 0.0 reduce-scatter.5.cloned.1.call-start
  273.5 0.0 reduce-scatter.3.cloned.1.call-done
  273.6 1.2 fusion.33
  274.8 1.2 fusion.35
  276.0 2.4 all_gather.30
  278.3 366.6 %all-to-all-done = bf16[16,4096,128]{1,2,0:T(8,128)(2,1)} async-done(((bf16[16,4096,128]{1,2,0:T(8,128)(2,1)}), bf16[16,4096,128]{1,2,0:T(8,128)(2,1)}, u32[]{:S(2)}, u32[]{:S(2)}) %all-to-all-start) | async-done | bytes 16777248 | tf_op jit(solution)/shard_map/all_to_all | solution.py:134
  645.0 128.7 %all-gather.16.cloned.1.call-done = bf16[2048,4096]{1,0:T(8,128)(2,1)} async-done(((bf16[128,4096]{1,0:T(8,128)(2,1)}), bf16[2048,4096]{1,0:T(8,128)(2,1)}) %all-gather.16.cloned.1.call-update) | async-done | bytes 16777232 | tf_op jit(solution)/shard_map/all_gather | solution.py:127
  773.7 16.2 %convolution_convert_fusion = bf16[192,2048]{1,0:T(8,128)(2,1)} fusion(bf16[4096,2048]{0,1:T(8,128)(2,1)} %bitcast.19, bf16[192,2048]{1,0:T(8,128)(2,1)S(1)} %all_gather.30, bf16[2048,4096]{1,0:T(8,128)(2,1)} %all-gather.16.cloned.1.call-done), kind=kOutput, calls=%fused_computation.18 | convolution fusion | flops 6445203456 | bytes 35127296 | tf_op jit(solution)/shard_map/dot_general | solution.py:131
  789.9 40.8 %reduce-scatter.5.cloned.1.call-done = bf16[96,2048]{1,0:T(8,128)(2,1)} async-done(((bf16[192,2048]{1,0:T(8,128)(2,1)}), bf16[96,2048]{1,0:T(8,128)(2,1)}) %reduce-scatter.5.cloned.1.call-update) | async-done | bytes 393232 | tf_op jit(solution)/shard_map/reduce_scatter | solution.py:138
  830.7 1.9 fusion.36
  (50 shorter events, 0.2 us)
Async XLA Ops:
  6.5 197.3 %copy-start = (bf16[256,2048]{1,0:T(8,128)(2,1)S(1)}, bf16[256,2048]{1,0:T(8,128)(2,1)}, u32[]{:S(2)}) copy-start(bf16[256,2048]{1,0:T(8,128)(2,1)} %param.23) | copy-start | bytes 3145732
  6.5 88.1 %all-gather.8.cloned.1.call-start = ((), (), s32[]{:S(2)}) async-start(), calls=%async_computation.3 | async-start | bytes 1671168 | tf_op jit(solution)/shard_map/all_gather | solution.py:85
  7.3 123.3 %all-gather.12.cloned.1.call-start = ((), (), s32[]{:S(2)}) async-start(), calls=%async_computation.5 | async-start | bytes 1671168 | tf_op jit(solution)/shard_map/all_gather | solution.py:87
  8.0 182.0 %all-gather.10.cloned.1.call-start = ((), (), s32[]{:S(2)}) async-start(), calls=%async_computation.4 | async-start | bytes 1671168 | tf_op jit(solution)/shard_map/all_gather | solution.py:86
  8.7 240.7 %all-gather.14.cloned.1.call-start = ((), (), s32[]{:S(2)}) async-start(), calls=%async_computation.6 | async-start | bytes 1671168 | tf_op jit(solution)/shard_map/all_gather | solution.py:88
  9.3 264.2 %reduce-scatter.3.cloned.1.call-start = ((), (), s32[]{:S(2)}) async-start(), calls=%async_computation.7 | async-start | bytes 1179648 | tf_op jit(solution)/shard_map/reduce_scatter | solution.py:114
  10.7 94.0 %copy-start.2 = (f32[192,3072]{1,0:T(8,128)}, f32[192,3072]{1,0:T(8,128)S(1)}, u32[]{:S(2)}) copy-start(f32[192,3072]{1,0:T(8,128)S(1)} %get-tuple-element.6) | copy-start | bytes 7077892
  97.3 14.2 %copy-start.8 = (pred[192,3072]{1,0:T(8,128)(4,1)S(1)}, pred[192,3072]{1,0:T(8,128)(4,1)}, u32[]{:S(2)}) copy-start(pred[192,3072]{1,0:T(8,128)(4,1)} %get-tuple-element.5) | copy-start | bytes 1769476
  97.3 14.2 %copy-start.11 = (f32[3072,8]{0,1:T(8,128)S(1)}, f32[3072,8]{0,1:T(8,128)}, u32[]{:S(2)}) copy-start(f32[3072,8]{0,1:T(8,128)} %reshape.102) | copy-start | bytes 294916
  97.3 14.2 %copy-start.12 = (f32[192,8]{0,1:T(8,128)S(1)}, f32[192,8]{0,1:T(8,128)}, u32[]{:S(2)}) copy-start(f32[192,8]{0,1:T(8,128)} %param.21) | copy-start | bytes 18436
  104.7 6.4 copy-start.4
  104.7 6.8 copy-start.14
  133.2 59.6 %copy-start.9 = (pred[192,3072]{1,0:T(8,128)(4,1)S(1)}, pred[192,3072]{1,0:T(8,128)(4,1)}, u32[]{:S(2)}) copy-start(pred[192,3072]{1,0:T(8,128)(4,1)} %get-tuple-element.5) | copy-start | bytes 1769476
  133.2 59.6 %copy-start.13 = (f32[192,8]{0,1:T(8,128)S(1)}, f32[192,8]{0,1:T(8,128)}, u32[]{:S(2)}) copy-start(f32[192,8]{0,1:T(8,128)} %param.21) | copy-start | bytes 18436
  133.2 59.6 %copy-start.15 = (f32[8,192]{1,0:T(8,128)S(1)}, f32[8,192]{1,0:T(8,128)}, u32[]{:S(2)}) copy-start(f32[8,192]{1,0:T(8,128)} %copy-done.14) | copy-start | bytes 18436
  133.2 59.6 %copy-start.17 = (f32[8,192]{1,0:T(8,128)S(1)}, f32[8,192]{1,0:T(8,128)}, u32[]{:S(2)}) copy-start(f32[8,192]{1,0:T(8,128)} %fusion) | copy-start | bytes 18436
  190.1 15.4 %slice-start = ((s8[9437184]{0:T(1024)(128)(4,1)}), s8[1048576]{0:T(1024)(128)(4,1)S(1)}, s32[]{:S(2)}) async-start(s8[9437184]{0:T(1024)(128)(4,1)} %bitcast.48), calls=%async_computation.10 | async-start | bytes 2097152
  192.8 12.6 %slice-start.1 = ((s8[9437184]{0:T(1024)(128)(4,1)}), s8[4194304]{0:T(1024)(128)(4,1)S(1)}, s32[]{:S(2)}) async-start(s8[9437184]{0:T(1024)(128)(4,1)} %bitcast.48), calls=%async_computation.11 | async-start | bytes 8388608
  192.8 12.6 %slice-start.2 = ((s8[9437184]{0:T(1024)(128)(4,1)}), s8[4194304]{0:T(1024)(128)(4,1)S(1)}, s32[]{:S(2)}) async-start(s8[9437184]{0:T(1024)(128)(4,1)} %bitcast.48), calls=%async_computation.12 | async-start | bytes 8388608
  192.8 12.6 %copy-start.3 = (f32[192,3072]{1,0:T(8,128)S(1)}, f32[192,3072]{1,0:T(8,128)}, u32[]{:S(2)}) copy-start(f32[192,3072]{1,0:T(8,128)} %copy-done.2) | copy-start | bytes 7077892
  207.3 51.4 %copy-start.5 = (f32[192,2048]{1,0:T(8,128)S(1)}, f32[192,2048]{1,0:T(8,128)}, u32[]{:S(2)}) copy-start(f32[192,2048]{1,0:T(8,128)} %fusion.42) | copy-start | bytes 4718596
  207.3 51.4 %copy-start.10 = (bf16[256,2048]{1,0:T(8,128)(2,1)S(1)}, bf16[256,2048]{1,0:T(8,128)(2,1)}, u32[]{:S(2)}) copy-start(bf16[256,2048]{1,0:T(8,128)(2,1)} %param.24) | copy-start | bytes 3145732
  267.6 6.0 copy-start.6
  267.6 7.2 copy-start.16
  267.6 377.4 %all-to-all-start = ((bf16[16,4096,128]{1,2,0:T(8,128)(2,1)}), bf16[16,4096,128]{1,2,0:T(8,128)(2,1)}, u32[]{:S(2)}, u32[]{:S(2)}) async-start(bf16[16,4096,128]{1,2,0:T(8,128)(2,1)} %stack.2), calls=%async_computation.1 | async-start | bytes 33554432 | tf_op jit(solution)/shard_map/all_to_all | solution.py:134
  272.9 500.8 %all-gather.16.cloned.1.call-start = ((), (), s32[]{:S(2)}) async-start(), calls=%async_computation.8 | async-start | bytes 17825792 | tf_op jit(solution)/shard_map/all_gather | solution.py:127
  273.5 557.2 %reduce-scatter.5.cloned.1.call-start = ((), (), s32[]{:S(2)}) async-start(), calls=%async_computation.9 | async-start | bytes 1179648 | tf_op jit(solution)/shard_map/reduce_scatter | solution.py:138
  773.7 57.0 %copy-start.7 = (bf16[96,2048]{1,0:T(8,128)(2,1)S(1)}, bf16[96,2048]{1,0:T(8,128)(2,1)}, u32[]{:S(2)}) copy-start(bf16[96,2048]{1,0:T(8,128)(2,1)} %reduce-scatter.3.cloned.1.call-done) | copy-start | bytes 1179652
  773.7 58.9 %copy-start.1 = (bf16[256,2048]{1,0:T(8,128)(2,1)S(1)}, bf16[256,2048]{1,0:T(8,128)(2,1)}, u32[]{:S(2)}) copy-start(bf16[256,2048]{1,0:T(8,128)(2,1)} %param.23) | copy-start | bytes 3145732
Sparse Core Ops, SparseCore 0:
  10.1 60.9 all-gather.7
  73.8 56.6 all-gather.11
  133.3 56.6 all-gather.9
  192.7 56.7 all-gather.13
  260.2 6.8 reduce-scatter.2
  276.2 497.4 all-gather.15
  790.0 40.5 reduce-scatter.4
